TPU v7x, 512 devices: a whole 4x8x8 slice. The times are simulated.
512 devices in a mesh: fs: 64 (over z, y), tp: 8 (over x, core).
Axes of the slice: x: 4, y: 8, z: 8, core: 2. Of those that a mesh axis runs over, the one named last changes fastest.
Arguments:
- late_input: bfloat16 [8192, 2048], P('fs', 'tp'), may hold values from -6 to 6
- up_weight: bfloat16 [2048, 4096], P('tp', 'fs'), may hold values from -0.125 to 0.125
- down_weight: bfloat16 [4096, 2048], P('fs', 'tp'), may hold values from -0.09375 to 0.09375
- early_input: bfloat16 [8192, 2048], P('fs', 'tp'), may hold values from -6 to 6
- early_pre: bfloat16 [8192, 4096], P('fs'), may hold values from -6 to 6
- cotangent: bfloat16 [8192, 2048], P('fs', 'tp'), may hold values from -16 to 16
- up_sum: float32 [2048, 4096], P('tp', 'fs'), may hold values from -24 to 24
- down_sum: float32 [4096, 2048], P('fs', 'tp'), may hold values from -24 to 24
Outputs:
- late_pre: bfloat16 [8192, 4096], P('fs')
- late_out: bfloat16 [8192, 2048], P('fs', 'tp')
- input_grad: bfloat16 [8192, 2048], P('fs', 'tp')
- up_total: float32 [2048, 4096], P('tp', 'fs')
- down_total: float32 [4096, 2048], P('fs', 'tp')
All inputs are finite; a program needn't handle non-finite values.
Results may differ from a plain program's by a relative error of at most 0.025.
Values may be sent and summed in bfloat16 or wider, within the bound.
A program may use at most 128 MiB of HBM per device.

v0:
```python
import jax
import jax.numpy as jnp
from jax import lax
from jax.sharding import Mesh
from jax.sharding import PartitionSpec as P

FS = ("fs_0", "fs_1")


def gathered_total(shard, axis):
    parts = lax.all_gather(shard, axis).astype(jnp.float32)
    return parts.sum(axis=0)


def own_rows(so_far, axes):
    for axis in axes:
        so_far = lax.psum_scatter(so_far, axis, scatter_dimension=0, tiled=True)
    return so_far


def contract_rows(left, right):
    return lax.dot_general(
        left, right, (((0,), (0,)), ((), ())), preferred_element_type=jnp.float32
    )


def contract_cols(left, right):
    return lax.dot_general(
        left, right, (((1,), (1,)), ((), ())), preferred_element_type=jnp.float32
    )


def body(late_input, up_weight, down_weight, early_input, early_pre, cotangent, up_sum, down_sum):
    up_gathered = lax.all_gather(up_weight, FS, axis=1, tiled=True)
    down_gathered = lax.all_gather(down_weight, FS, axis=0, tiled=True)
    pre_terms = jnp.dot(late_input, up_gathered, preferred_element_type=jnp.float32)
    pre_summed = gathered_total(pre_terms.astype(jnp.bfloat16), "tp").astype(jnp.float32)
    late_pre = pre_summed.astype(jnp.bfloat16)
    late_hidden = jnp.square(jax.nn.relu(late_pre.astype(jnp.float32))).astype(jnp.bfloat16)
    early_float = early_pre.astype(jnp.float32)
    early_hidden = jnp.square(jax.nn.relu(early_float)).astype(jnp.bfloat16)
    late_out = jnp.dot(late_hidden, down_gathered, preferred_element_type=jnp.float32).astype(
        jnp.bfloat16
    )
    grad_terms = contract_cols(cotangent, down_gathered)
    hidden_grad = gathered_total(grad_terms.astype(jnp.bfloat16), "tp").astype(jnp.float32)
    pre_grad = (hidden_grad * 2.0 * jax.nn.relu(early_float)).astype(jnp.bfloat16)
    input_grad = contract_cols(pre_grad, up_gathered).astype(jnp.bfloat16)
    grad_local = lax.all_to_all(pre_grad, FS, split_axis=1, concat_axis=0, tiled=True)
    up_grad = contract_rows(lax.all_gather(early_input, FS, axis=0, tiled=True), grad_local)
    up_total = up_sum + up_grad
    down_grad = own_rows(contract_rows(early_hidden, cotangent), FS)
    down_total = down_sum + down_grad
    return (late_pre, late_out, input_grad, up_total, down_total)


def solution(mesh):
    split = Mesh(mesh.devices.reshape(8, 8, mesh.shape["tp"]), ("fs_0", "fs_1", "tp"))
    placed = (
        P(FS, "tp"),
        P("tp", FS),
        P(FS, "tp"),
        P(FS, "tp"),
        P(FS, None),
        P(FS, "tp"),
        P("tp", FS),
        P(FS, "tp"),
    )
    return jax.shard_map(
        body,
        mesh=split,
        in_specs=placed,
        out_specs=(P(FS, None), P(FS, "tp"), P(FS, "tp"), P("tp", FS), P(FS, "tp")),
        check_vma=False,
    )
```

profile of v0, /device:TPU:2, one launch (start us, length us, event | category | flops | bytes accessed | tf_op | source)
XLA Modules:
  0.0 414.4 jit_solution(17327344246205105072)
XLA Ops:
  8.0 0.0 all-gather.10.cloned.1.call-start
  8.1 0.7 all-gather.10.cloned.1.call-update
  8.7 0.0 reduce-scatter.3.cloned.1.call-start
  8.8 0.0 copy-done
  8.8 3.9 fusion.1
  12.8 0.0 all-gather.8.cloned.1.call-start
  12.8 0.7 all-gather.8.cloned.1.call-update
  13.6 0.0 all-gather.16.cloned.1.call-start
  13.6 104.6 %all-gather.10.cloned.1.call-done = bf16[4096,256]{1,0:T(8,128)(2,1)} async-done(((bf16[64,256]{1,0:T(8,128)(2,1)}), bf16[4096,256]{1,0:T(8,128)(2,1)}) %all-gather.10.cloned.1.call-update) | async-done | bytes 2097168 | tf_op jit(solution)/shard_map/all_gather | solution.py:35
  118.2 3.5 convolution_convert_fusion
  121.6 0.0 reduce-scatter.5.cloned.1.call-start
  121.7 0.5 reduce-scatter.5.cloned.1.call-update
  122.2 0.0 all-gather.14.cloned.1.call-start
  122.3 79.3 %all-gather.8.cloned.1.call-done = bf16[256,4096]{0,1:T(8,128)(2,1)} async-done(((bf16[256,64]{0,1:T(8,128)(2,1)}), bf16[256,4096]{0,1:T(8,128)(2,1)}) %all-gather.8.cloned.1.call-update) | async-done | bytes 2097168 | tf_op jit(solution)/shard_map/all_gather | solution.py:34
  201.6 3.4 convolution_convert_fusion.1
  205.0 0.0 all-gather.12.cloned.1.call-start
  205.0 0.5 all-gather.12.cloned.1.call-update
  205.6 49.1 %all-gather.16.cloned.1.call-done = bf16[1024,4096]{1,0:T(8,128)(2,1)} async-done(((bf16[128,4096]{1,0:T(8,128)(2,1)}), bf16[1024,4096]{1,0:T(8,128)(2,1)}) %all-gather.16.cloned.1.call-update) | async-done | bytes 8388624 | tf_op jit(solution)/shard_map/all_gather | solution.py:11
  254.7 5.1 %convert_reduce_fusion = f32[128,4096]{1,0:T(8,128)S(1)} fusion(bf16[8,128,4096]{2,1,0:T(8,128)(2,1)} %bitcast.25), kind=kLoop, calls=%fused_computation | loop fusion | flops 7864320 | bytes 10485760 | tf_op jit(solution)/shard_map/reduce_sum | solution.py:12
  259.9 0.3 multiply_convert_fusion.1
  260.2 1.3 copy.16
  261.5 13.5 %all-to-all-start = ((bf16[128,64,64]{0,2,1:T(8,128)(2,1)}), bf16[128,64,64]{0,2,1:T(8,128)(2,1)}, u32[]{:S(2)}, u32[]{:S(2)}) async-start(bf16[128,64,64]{0,2,1:T(8,128)(2,1)} %bitcast.2), calls=%async_computation | async-start | bytes 2097152 | tf_op jit(solution)/shard_map/all_to_all | solution.py:49
  275.1 0.0 reduce-scatter.5.cloned.1.call-done
  275.1 1.5 add.11
  276.6 35.9 %all-gather.14.cloned.1.call-done = bf16[1024,4096]{1,0:T(8,128)(2,1)} async-done(((bf16[128,4096]{1,0:T(8,128)(2,1)}), bf16[1024,4096]{1,0:T(8,128)(2,1)}) %all-gather.14.cloned.1.call-update) | async-done | bytes 8388624 | tf_op jit(solution)/shard_map/all_gather | solution.py:11
  312.5 6.2 %reduce_sum.21 = bf16[128,4096]{1,0:T(8,128)(2,1)} reduce(bf16[8,128,4096]{2,1,0:T(8,128)(2,1)} %bitcast.26, bf16[]{:T(256)} %constant.7.clone.1), dimensions={0}, to_apply=%region_0.0 | reduce | flops 3670016 | bytes 9437186 | tf_op jit(solution)/shard_map/reduce_sum | solution.py:12
  318.7 1.1 convolution_convert_fusion.2
  319.8 0.5 copy-done.3
  320.4 0.3 copy-done.4
  320.6 1.1 convolution_convert_fusion.3
  321.7 81.6 %all-gather.12.cloned.1.call-done = bf16[8192,256]{1,0:T(8,128)(2,1)} async-done(((bf16[128,256]{1,0:T(8,128)(2,1)}), bf16[8192,256]{1,0:T(8,128)(2,1)}) %all-gather.12.cloned.1.call-update) | async-done | bytes 4194320 | tf_op jit(solution)/shard_map/all_gather | solution.py:50
  403.3 4.0 fusion
  (18 shorter events, 0.1 us)
Async XLA Ops:
  8.0 0.8 copy-start
  8.0 110.1 %all-gather.10.cloned.1.call-start = ((), (), s32[]{:S(2)}) async-start(), calls=%async_computation.4 | async-start | bytes 2129920 | tf_op jit(solution)/shard_map/all_gather | solution.py:35
  8.7 113.0 %reduce-scatter.3.cloned.1.call-start = ((), (), s32[]{:S(2)}) async-start(), calls=%async_computation.6 | async-start | bytes 4718592 | tf_op jit(solution)/shard_map/reduce_scatter | solution.py:17
  12.8 188.8 %all-gather.8.cloned.1.call-start = ((), (), s32[]{:S(2)}) async-start(), calls=%async_computation.3 | async-start | bytes 2129920 | tf_op jit(solution)/shard_map/all_gather | solution.py:34
  13.5 188.0 %copy-start.6 = (bf16[128,256]{1,0:T(8,128)(2,1)S(1)}, bf16[128,256]{1,0:T(8,128)(2,1)}, u32[]{:S(2)}) copy-start(bf16[128,256]{1,0:T(8,128)(2,1)} %param.8) | copy-start | bytes 196612
  13.6 241.2 %all-gather.16.cloned.1.call-start = ((), (), s32[]{:S(2)}) async-start(), calls=%async_computation.9 | async-start | bytes 9437184 | tf_op jit(solution)/shard_map/all_gather | solution.py:11
  121.6 153.5 %reduce-scatter.5.cloned.1.call-start = ((), (), s32[]{:S(2)}) async-start(), calls=%async_computation.7 | async-start | bytes 589824 | tf_op jit(solution)/shard_map/reduce_scatter | solution.py:17
  122.2 190.3 %all-gather.14.cloned.1.call-start = ((), (), s32[]{:S(2)}) async-start(), calls=%async_computation.8 | async-start | bytes 9437184 | tf_op jit(solution)/shard_map/all_gather | solution.py:11
  205.0 198.3 %all-gather.12.cloned.1.call-start = ((), (), s32[]{:S(2)}) async-start(), calls=%async_computation.5 | async-start | bytes 4259840 | tf_op jit(solution)/shard_map/all_gather | solution.py:50
  254.7 5.1 %copy-start.2 = (bf16[128,4096]{1,0:T(8,128)(2,1)S(1)}, bf16[128,4096]{1,0:T(8,128)(2,1)}, u32[]{:S(2)}) copy-start(bf16[128,4096]{1,0:T(8,128)(2,1)} %param.12) | copy-start | bytes 3145732
  260.2 14.9 %copy-start.7 = (f32[64,256]{1,0:T(8,128)S(1)}, f32[64,256]{1,0:T(8,128)}, u32[]{:S(2)}) copy-start(f32[64,256]{1,0:T(8,128)} %param.15) | copy-start | bytes 196612
  261.5 141.8 %all-to-all-start = ((bf16[128,64,64]{0,2,1:T(8,128)(2,1)}), bf16[128,64,64]{0,2,1:T(8,128)(2,1)}, u32[]{:S(2)}, u32[]{:S(2)}) async-start(bf16[128,64,64]{0,2,1:T(8,128)(2,1)} %bitcast.2), calls=%async_computation | async-start | bytes 2097152 | tf_op jit(solution)/shard_map/all_to_all | solution.py:49
  312.5 6.2 %copy-start.1 = (bf16[256,4096]{0,1:T(8,128)(2,1)S(1)}, bf16[256,4096]{0,1:T(8,128)(2,1)}, u32[]{:S(2)}) copy-start(bf16[256,4096]{0,1:T(8,128)(2,1)} %all-gather.8.cloned.1.call-done) | copy-start | bytes 6291460
  318.7 1.6 copy-start.3
  318.7 1.9 copy-start.4
  320.6 82.7 %copy-start.5 = (f32[256,64]{0,1:T(8,128)S(1)}, f32[256,64]{0,1:T(8,128)}, u32[]{:S(2)}) copy-start(f32[256,64]{0,1:T(8,128)} %param.14) | copy-start | bytes 196612
Sparse Core Ops, SparseCore 0:
  11.9 106.2 all-gather.9
  121.2 80.3 all-gather.7
  203.7 50.9 all-gather.15
  257.3 55.1 all-gather.13
  315.4 87.8 all-gather.11
Sparse Core Ops, SparseCore 1:
  12.9 64.5 reduce-scatter.2
  124.9 36.8 reduce-scatter.4
where the time goes:
time: 415 us; the launch traced here: 414 us
  waiting for transfers between devices  353 us (85%)
  matrix products  16.9 us (4%)
  between operations  15.3 us (4%)
  starting transfers between devices  13.8 us (3%)
  other arithmetic  13.2 us (3%)
    all_gather x1, waiting for transfers between devices, body(): down_gathered = lax.all_gather(down_weight, FS, axis=0, tiled=True)  105 us
    all_gather x2, waiting for transfers between devices, gathered_total(): parts = lax.all_gather(shard, axis).astype(jnp.float32)  85 us
    all_gather x1, waiting for transfers between devices, body(): lax.all_gather(early_input, FS, axis=0, tiled=True)  81.6 us
    all_gather x1, waiting for transfers between devices, body(): up_gathered = lax.all_gather(up_weight, FS, axis=1, tiled=True)  79.3 us
    all_to_all x1, starting transfers between devices, body(): lax.all_to_all(pre_grad, FS, split_axis=1, concat_axis=0, tiled=True)  13.5 us
    reduce_sum x2, other arithmetic, gathered_total(): return parts.sum(axis=0)  11.3 us
  transfers between devices with their start and end apart: 8, of which 5 were waited for; matrix products, arithmetic and copies ran while one was open for 7% of the time, Pallas kernels for 0%

commit v1 on v0

--- a/solution.py
+++ b/solution.py
@@ -47,7 +47,18 @@
     pre_grad = (hidden_grad * 2.0 * jax.nn.relu(early_float)).astype(jnp.bfloat16)
     input_grad = contract_cols(pre_grad, up_gathered).astype(jnp.bfloat16)
     grad_local = lax.all_to_all(pre_grad, FS, split_axis=1, concat_axis=0, tiled=True)
-    up_grad = contract_rows(lax.all_gather(early_input, FS, axis=0, tiled=True), grad_local)
+    up_grad = contract_rows(
+        jnp.concatenate(
+            lax.all_to_all(
+                jnp.stack(lax.axis_size(FS) * [early_input], axis=0),
+                axis_name=FS,
+                split_axis=0,
+                concat_axis=0,
+            ),
+            axis=0,
+        ),
+        grad_local,
+    )
     up_total = up_sum + up_grad
     down_grad = own_rows(contract_rows(early_hidden, cotangent), FS)
     down_total = down_sum + down_grad

time: 415 us -> 373 us (0.90)
  the two profiles are of different devices: /device:TPU:2 before, /device:TPU:8 now
where the time goes in v1:
time: 373 us
  waiting for transfers between devices  288 us (77%)
  starting transfers between devices  34.5 us (9%)
  matrix products  16.9 us (5%)
  between operations  15.3 us (4%)
  other arithmetic  13.1 us (4%)
  local copies, waits for them, and re-layouts  4.73 us (1%)
    all_gather x1, waiting for transfers between devices, body(): down_gathered = lax.all_gather(down_weight, FS, axis=0, tiled=True)  104 us
    all_gather x1, waiting for transfers between devices, body(): up_gathered = lax.all_gather(up_weight, FS, axis=1, tiled=True)  79.3 us
    all_to_all x1, waiting for transfers between devices, body(): lax.all_to_all(jnp.stack(lax.axis_size(FS) * [early_input], axis=0), axis...  49.4 us
    all_gather x2, waiting for transfers between devices, gathered_total(): parts = lax.all_gather(shard, axis).astype(jnp.float32)  39 us
    all_to_all x1, starting transfers between devices, body(): lax.all_to_all(pre_grad, FS, split_axis=1, concat_axis=0, tiled=True)  24.7 us
    all_to_all x1, waiting for transfers between devices, body(): lax.all_to_all(pre_grad, FS, split_axis=1, concat_axis=0, tiled=True)  14.4 us
    reduce_sum x2, other arithmetic, gathered_total(): return parts.sum(axis=0)  11.3 us
    all_to_all x1, starting transfers between devices, body(): lax.all_to_all(jnp.stack(lax.axis_size(FS) * [early_input], axis=0), axis...  9.51 us
  transfers between devices with their start and end apart: 8, of which 5 were waited for; matrix products, arithmetic and copies ran while one was open for 8% of the time, Pallas kernels for 0%

profile of v1, /device:TPU:8, one launch (start us, length us, event | category | flops | bytes accessed | tf_op | source)
XLA Modules:
  0.0 372.5 jit_solution(10098644241287315383)
XLA Ops:
  8.0 0.0 all-gather.9.cloned.1.call-start
  8.1 0.7 all-gather.9.cloned.1.call-update
  8.7 0.0 reduce-scatter.3.cloned.1.call-start
  8.8 0.0 copy-done
  8.8 3.9 %fusion.1 = f32[4096,256]{1,0:T(8,128)} fusion(bf16[128,256]{1,0:T(8,128)(2,1)S(1)} %copy-done, bf16[128,4096]{1,0:T(8,128)(2,1)} %param.12), kind=kOutput, calls=%fused_computation.11 | convolution fusion | flops 270532608 | bytes 5308416 | tf_op jit(solution)/shard_map/dot_general | solution.py:22
  12.8 0.0 all-gather.7.cloned.1.call-start
  12.8 0.7 all-gather.7.cloned.1.call-update
  13.6 0.0 all-gather.13.cloned.1.call-start
  13.6 104.0 %all-gather.9.cloned.1.call-done = bf16[4096,256]{1,0:T(8,128)(2,1)} async-done(((bf16[64,256]{1,0:T(8,128)(2,1)}), bf16[4096,256]{1,0:T(8,128)(2,1)}) %all-gather.9.cloned.1.call-update) | async-done | bytes 2097168 | tf_op jit(solution)/shard_map/all_gather | solution.py:35
  117.6 3.4 convolution_convert_fusion
  121.0 0.0 reduce-scatter.5.cloned.1.call-start
  121.1 0.5 reduce-scatter.5.cloned.1.call-update
  121.7 0.0 all-gather.11.cloned.1.call-start
  121.7 79.3 %all-gather.7.cloned.1.call-done = bf16[256,4096]{0,1:T(8,128)(2,1)} async-done(((bf16[256,64]{0,1:T(8,128)(2,1)}), bf16[256,4096]{0,1:T(8,128)(2,1)}) %all-gather.7.cloned.1.call-update) | async-done | bytes 2097168 | tf_op jit(solution)/shard_map/all_gather | solution.py:34
  201.0 3.4 convolution_convert_fusion.1
  204.4 2.5 stack.2
  206.9 9.5 %all-to-all-start.1 = ((bf16[64,128,256]{2,1,0:T(8,128)(2,1)}), bf16[64,128,256]{2,1,0:T(8,128)(2,1)}, u32[]{:S(2)}, u32[]{:S(2)}) async-start(bf16[64,128,256]{2,1,0:T(8,128)(2,1)} %stack.2), calls=%async_computation.1 | async-start | bytes 8388608 | tf_op jit(solution)/shard_map/all_to_all | solution.py:52
  216.4 39.0 %all-gather.13.cloned.1.call-done = bf16[1024,4096]{1,0:T(8,128)(2,1)} async-done(((bf16[128,4096]{1,0:T(8,128)(2,1)}), bf16[1024,4096]{1,0:T(8,128)(2,1)}) %all-gather.13.cloned.1.call-update) | async-done | bytes 8388624 | tf_op jit(solution)/shard_map/all_gather | solution.py:11
  255.4 5.1 %convert_reduce_fusion = f32[128,4096]{1,0:T(8,128)S(1)} fusion(bf16[8,128,4096]{2,1,0:T(8,128)(2,1)} %bitcast.22), kind=kLoop, calls=%fused_computation | loop fusion | flops 7864320 | bytes 10485760 | tf_op jit(solution)/shard_map/reduce_sum | solution.py:12
  260.6 0.3 multiply_convert_fusion.1
  260.9 1.4 copy.13
  262.2 49.4 %all-to-all-done.1 = bf16[64,128,256]{2,1,0:T(8,128)(2,1)} async-done(((bf16[64,128,256]{2,1,0:T(8,128)(2,1)}), bf16[64,128,256]{2,1,0:T(8,128)(2,1)}, u32[]{:S(2)}, u32[]{:S(2)}) %all-to-all-start.1) | async-done | bytes 4194336 | tf_op jit(solution)/shard_map/all_to_all | solution.py:52
  311.6 24.7 %all-to-all-start = ((bf16[128,64,64]{0,2,1:T(8,128)(2,1)}), bf16[128,64,64]{0,2,1:T(8,128)(2,1)}, u32[]{:S(2)}, u32[]{:S(2)}) async-start(bf16[128,64,64]{0,2,1:T(8,128)(2,1)} %bitcast.2), calls=%async_computation | async-start | bytes 2097152 | tf_op jit(solution)/shard_map/all_to_all | solution.py:49
  336.3 0.0 reduce-scatter.5.cloned.1.call-done
  336.4 1.5 add.11
  337.8 6.2 %reduce_sum.21 = bf16[128,4096]{1,0:T(8,128)(2,1)} reduce(bf16[8,128,4096]{2,1,0:T(8,128)(2,1)} %bitcast.23, bf16[]{:T(256)} %constant.7.clone.1), dimensions={0}, to_apply=%region_0.0 | reduce | flops 3670016 | bytes 9437186 | tf_op jit(solution)/shard_map/reduce_sum | solution.py:12
  344.1 1.1 convolution_convert_fusion.2
  345.1 0.5 copy-done.3
  345.7 0.3 copy-done.4
  345.9 1.1 convolution_convert_fusion.3
  347.0 14.4 %all-to-all-done = bf16[128,64,64]{0,2,1:T(8,128)(2,1)} async-done(((bf16[128,64,64]{0,2,1:T(8,128)(2,1)}), bf16[128,64,64]{0,2,1:T(8,128)(2,1)}, u32[]{:S(2)}, u32[]{:S(2)}) %all-to-all-start) | async-done | bytes 1048608 | tf_op jit(solution)/shard_map/all_to_all | solution.py:49
  361.4 4.0 %fusion = f32[256,64]{0,1:T(8,128)} fusion(f32[256,64]{0,1:T(8,128)S(1)} %copy-done.6, bf16[64,128,256]{2,1,0:T(8,128)(2,1)} %all-to-all-done.1, bf16[128,64,64]{0,2,1:T(8,128)(2,1)} %all-to-all-done), kind=kOutput, calls=%fused_computation.10 | convolution fusion | flops 268451840 | bytes 5373952 | tf_op jit(solution)/shard_map/dot_general | solution.py:22
  (20 shorter events, 0.1 us)
Async XLA Ops:
  8.0 0.8 copy-start
  8.0 109.6 %all-gather.9.cloned.1.call-start = ((), (), s32[]{:S(2)}) async-start(), calls=%async_computation.5 | async-start | bytes 2129920 | tf_op jit(solution)/shard_map/all_gather | solution.py:35
  8.7 112.4 %reduce-scatter.3.cloned.1.call-start = ((), (), s32[]{:S(2)}) async-start(), calls=%async_computation.6 | async-start | bytes 4718592 | tf_op jit(solution)/shard_map/reduce_scatter | solution.py:17
  12.8 188.2 %all-gather.7.cloned.1.call-start = ((), (), s32[]{:S(2)}) async-start(), calls=%async_computation.4 | async-start | bytes 2129920 | tf_op jit(solution)/shard_map/all_gather | solution.py:34
  13.5 187.4 %copy-start.7 = (bf16[128,256]{1,0:T(8,128)(2,1)S(1)}, bf16[128,256]{1,0:T(8,128)(2,1)}, u32[]{:S(2)}) copy-start(bf16[128,256]{1,0:T(8,128)(2,1)} %param.8) | copy-start | bytes 196612
  13.6 241.8 %all-gather.13.cloned.1.call-start = ((), (), s32[]{:S(2)}) async-start(), calls=%async_computation.9 | async-start | bytes 9437184 | tf_op jit(solution)/shard_map/all_gather | solution.py:11
  121.0 215.3 %reduce-scatter.5.cloned.1.call-start = ((), (), s32[]{:S(2)}) async-start(), calls=%async_computation.7 | async-start | bytes 589824 | tf_op jit(solution)/shard_map/reduce_scatter | solution.py:17
  121.6 82.7 %copy-start.5 = (bf16[128,256]{1,0:T(8,128)(2,1)S(1)}, bf16[128,256]{1,0:T(8,128)(2,1)}, u32[]{:S(2)}) copy-start(bf16[128,256]{1,0:T(8,128)(2,1)} %param.11) | copy-start | bytes 196612
  121.7 216.2 %all-gather.11.cloned.1.call-start = ((), (), s32[]{:S(2)}) async-start(), calls=%async_computation.8 | async-start | bytes 9437184 | tf_op jit(solution)/shard_map/all_gather | solution.py:11
  206.9 104.7 %all-to-all-start.1 = ((bf16[64,128,256]{2,1,0:T(8,128)(2,1)}), bf16[64,128,256]{2,1,0:T(8,128)(2,1)}, u32[]{:S(2)}, u32[]{:S(2)}) async-start(bf16[64,128,256]{2,1,0:T(8,128)(2,1)} %stack.2), calls=%async_computation.1 | async-start | bytes 8388608 | tf_op jit(solution)/shard_map/all_to_all | solution.py:52
  255.4 5.1 %copy-start.2 = (bf16[128,4096]{1,0:T(8,128)(2,1)S(1)}, bf16[128,4096]{1,0:T(8,128)(2,1)}, u32[]{:S(2)}) copy-start(bf16[128,4096]{1,0:T(8,128)(2,1)} %param.12) | copy-start | bytes 3145732
  260.9 75.5 %copy-start.8 = (f32[64,256]{1,0:T(8,128)S(1)}, f32[64,256]{1,0:T(8,128)}, u32[]{:S(2)}) copy-start(f32[64,256]{1,0:T(8,128)} %param.15) | copy-start | bytes 196612
  311.6 49.8 %all-to-all-start = ((bf16[128,64,64]{0,2,1:T(8,128)(2,1)}), bf16[128,64,64]{0,2,1:T(8,128)(2,1)}, u32[]{:S(2)}, u32[]{:S(2)}) async-start(bf16[128,64,64]{0,2,1:T(8,128)(2,1)} %bitcast.2), calls=%async_computation | async-start | bytes 2097152 | tf_op jit(solution)/shard_map/all_to_all | solution.py:49
  337.8 6.2 %copy-start.1 = (bf16[256,4096]{0,1:T(8,128)(2,1)S(1)}, bf16[256,4096]{0,1:T(8,128)(2,1)}, u32[]{:S(2)}) copy-start(bf16[256,4096]{0,1:T(8,128)(2,1)} %all-gather.7.cloned.1.call-done) | copy-start | bytes 6291460
  344.0 1.6 copy-start.3
  344.1 1.9 copy-start.4
  345.9 15.5 %copy-start.6 = (f32[256,64]{0,1:T(8,128)S(1)}, f32[256,64]{0,1:T(8,128)}, u32[]{:S(2)}) copy-start(f32[256,64]{0,1:T(8,128)} %param.14) | copy-start | bytes 196612
Sparse Core Ops, SparseCore 0:
  11.9 105.6 all-gather.8
  120.7 80.2 all-gather.6
  203.1 52.2 all-gather.12
  258.0 55.1 all-gather.10
Sparse Core Ops, SparseCore 1:
  12.9 64.4 reduce-scatter.2
  124.3 36.9 reduce-scatter.4
